TPU v7x, 512 devices: a 4x2x32 block of a 4x8x32 slice. The times are simulated.
512 devices in a mesh: grp: 2 (over y), sp: 32 (over z), tp: 8 (over x, core).
Axes of the slice: x: 4, y: 2, z: 32, core: 2. Of those that a mesh axis runs over, the one named last changes fastest.
The devices are a block of a 4x8x32 slice.
Arguments:
- starting_stream: bfloat16 [24576, 2048], P(('grp', 'sp'), 'tp'), parts along dimension 0, may hold values from -45 to 45
- multiplier_matrix: bfloat16 [2, 2048, 2048], P(None, 'sp', 'tp'), may hold values from -0.125 to 0.125
- memory_path_matrix: bfloat16 [2, 2048, 2048], P(None, 'sp', 'tp'), may hold values from -0.125 to 0.125
- filter_coefficients: bfloat16 [2, 4, 2048], P(None, None, 'tp'), may hold values from -3 to 3
- memory_valve_matrix: bfloat16 [2, 8, 256, 256], P(None, 'tp'), may hold values from -0.375 to 0.375
- entry_valve_matrix: bfloat16 [2, 8, 256, 256], P(None, 'tp'), may hold values from -0.375 to 0.375
- forgetting_parameters: float32 [2, 2048], P(None, 'tp'), may hold values from 3 to 15
- timestep_forgetting_multiplier: float32 [24576], P(('grp', 'sp')), parts along dimension 0, may hold values from 0.5 to 2
- spike_extra: float32 [24576, 2048], P(('grp', 'sp'), 'tp'), parts along dimension 0, may hold values from -0.7 to 0
- exit_projector_matrix: bfloat16 [2, 2048, 2048], P(None, 'tp', 'sp'), may hold values from -0.125 to 0.125
- prelude_rms_gains: float32 [2, 2048], replicated, may hold values from 0.1 to 1.9
- finishing_rms_gains: float32 [2048], P('tp'), may hold values from 0.1 to 1.9
Outputs:
- result: bfloat16 [24576, 2048], P(('grp', 'sp'), 'tp'), parts along dimension 0
There are 2 independent parts, one for each index of `grp`. A program takes and returns all parts, laid end to end along the dimension named above; an argument that names none is the same for every part. Nothing has to cross between parts.
All inputs are finite; a program needn't handle non-finite values.
Results may differ from a plain program's by a relative error of at most 0.015.
Values may be sent and summed in bfloat16 or wider, within the bound.
A program may use at most 64 MiB of HBM per device.

v0:
```python
import jax
import jax.numpy as jnp
from jax import lax
from jax.sharding import PartitionSpec as P

BLOCK_W = 256


EPSILON = 1e-06
SQUASH_POWER = 8.0


def sent_to_all(x, axis):
    copies = jnp.broadcast_to(x, (lax.axis_size(axis), *x.shape))
    return lax.all_to_all(copies, axis, split_axis=0, concat_axis=0, tiled=True)


def laid_out(tiles, dim):
    lengths = list(tiles.shape[1:])
    lengths[dim] *= tiles.shape[0]
    return jnp.moveaxis(tiles, 0, dim).reshape(lengths)


def gather_directly(x, axis, dim):
    tiles = sent_to_all(x, axis)
    return laid_out(tiles, dim)


def in_one_piece(arrays, axis, dim, along):
    widths = [a.shape[along] for a in arrays]
    both = jnp.concatenate(arrays, axis=along)
    whole = lax.all_gather(both, axis, axis=dim, tiled=True)
    return tuple(jnp.split(whole, [sum(widths[:k]) for k in range(1, len(widths))], axis=along))


def from_behind(value, axis, steps):
    count = lax.axis_size(axis)
    first, last = (max(0, -steps), min(count, count - steps))
    return lax.ppermute(value, axis, [(source, source + steps) for source in range(first, last)])


def gathered_once(x, axis):
    leaves = jax.tree.leaves(x)
    turns = sorted(range(len(leaves)), key=lambda k: -leaves[k].size)
    width = (1, *leaves[turns[0]].shape)[-1]
    lines = [
        jnp.pad(leaves[k].reshape(-1), (0, -leaves[k].size % width)).reshape(-1, width)
        for k in turns
    ]
    both, at, found = (lax.all_gather(jnp.concatenate(lines), axis), 0, {})
    for k, line in zip(turns, lines):
        slab = both[:, at : at + len(line)].reshape(len(both), -1)
        found[k] = slab[:, : leaves[k].size].reshape(-1, *leaves[k].shape)
        at += len(line)
    numbers = iter(range(len(leaves)))
    return jax.tree.map(lambda _: found[next(numbers)], x)


def carried_in(part, axis, combine, identity):
    place = lax.axis_index(axis)
    gathered = gathered_once(part, axis)
    state = jax.tree.map(lambda a, e: jnp.zeros_like(a) + jnp.asarray(e, a.dtype), part, identity)

    def one(lap, state):
        return combine(
            state, jax.tree.map(lambda a: lax.dynamic_index_in_dim(a, lap, 0, False), gathered)
        )

    return lax.fori_loop(0, place, one, state)


def split_up(x, dim, count):
    before, after = (x.shape[:dim], x.shape[dim + 1 :])
    return jnp.moveaxis(x.reshape(*before, count, -1, *after), dim, 0)


def summed_on_arrival(x, axis, dim):
    tiles = split_up(x, dim, lax.axis_size(axis))
    arrived = lax.all_to_all(tiles, axis, split_axis=0, concat_axis=0, tiled=True)
    return arrived.astype(jnp.float32).sum(axis=0)


def of_everyone(x, axis):
    everything = sent_to_all(x, axis)
    return jnp.sum(everything, axis=0)


def combine_pairs(earlier, later):
    return (earlier[0] * later[0], later[0] * earlier[1] + later[1])


def gather_rows(own_cols):
    return gather_directly(own_cols, "tp", 1)


def fetch_layer(multiplier_matrix, memory_path_matrix, exit_projector_matrix, tier_number):
    in_pair = in_one_piece(
        (multiplier_matrix[tier_number], memory_path_matrix[tier_number]), "sp", 0, 1
    )
    out_full = lax.all_gather(exit_projector_matrix[tier_number], "sp", axis=1, tiled=True)
    return (in_pair[0], in_pair[1], out_full)


def on_device(
    starting_stream,
    multiplier_matrix,
    memory_path_matrix,
    filter_coefficients,
    memory_valve_matrix,
    entry_valve_matrix,
    forgetting_parameters,
    timestep_forgetting_multiplier,
    spike_extra,
    exit_projector_matrix,
    prelude_rms_gains,
    finishing_rms_gains,
):
    tok_rows = starting_stream.shape[0]
    channels = memory_path_matrix.shape[2]
    own_cols = starting_stream
    full_rows = gather_rows(starting_stream)
    fetched = fetch_layer(multiplier_matrix, memory_path_matrix, exit_projector_matrix, 0)
    for tier_number in range(memory_path_matrix.shape[0]):
        floats = full_rows.astype(jnp.float32)
        mean_square = jnp.mean(floats * floats, axis=1, keepdims=True)
        normed = (
            floats * lax.rsqrt(mean_square + EPSILON) * prelude_rms_gains[tier_number][None, :]
        ).astype(jnp.bfloat16)
        branch_acc = jnp.dot(normed, fetched[0], preferred_element_type=jnp.float32)
        recur_acc = jnp.dot(normed, fetched[1], preferred_element_type=jnp.float32)
        out_full = fetched[2]
        if tier_number + 1 < memory_path_matrix.shape[0]:
            fetched = fetch_layer(
                multiplier_matrix, memory_path_matrix, exit_projector_matrix, tier_number + 1
            )
        branch = branch_acc.astype(jnp.bfloat16)
        recurrent = recur_acc.astype(jnp.bfloat16)
        taps_now = filter_coefficients[tier_number]
        reach_back = taps_now.shape[0] - 1
        halo_rows = from_behind(recurrent[tok_rows - reach_back :], "sp", 1)
        extended = jnp.concatenate([halo_rows, recurrent], axis=0)
        conv_sum = jnp.zeros((tok_rows, channels), jnp.float32)
        for offset in range(taps_now.shape[0]):
            conv_sum = conv_sum + extended[offset : offset + tok_rows].astype(
                jnp.float32
            ) * taps_now[offset].astype(jnp.float32)
        convolved = conv_sum.astype(jnp.bfloat16)
        blocks = convolved.reshape(tok_rows, channels // BLOCK_W, BLOCK_W)
        reset_gate = jax.nn.sigmoid(
            jnp.einsum(
                "tnc,ncd->tnd",
                blocks,
                memory_valve_matrix[tier_number],
                preferred_element_type=jnp.float32,
            ).reshape(tok_rows, channels)
        )
        inject = jax.nn.sigmoid(
            jnp.einsum(
                "tnc,ncd->tnd",
                blocks,
                entry_valve_matrix[tier_number],
                preferred_element_type=jnp.float32,
            ).reshape(tok_rows, channels)
        )
        logarithmic_persistence = (
            -SQUASH_POWER
            * reset_gate
            * jax.nn.softplus(-forgetting_parameters[tier_number])[None, :]
            * timestep_forgetting_multiplier[:, None]
            + spike_extra
        )
        keep_rate = jnp.exp(logarithmic_persistence)
        driven = (
            inject
            * convolved.astype(jnp.float32)
            * jnp.sqrt(-jnp.expm1(2.0 * logarithmic_persistence))
        )
        keep_cum, state_local = lax.associative_scan(combine_pairs, (keep_rate, driven), axis=0)
        identity = (jnp.ones((channels,), jnp.float32), jnp.zeros((channels,), jnp.float32))
        carried = carried_in((keep_cum[-1], state_local[-1]), "sp", combine_pairs, identity)
        state_seq = state_local + keep_cum * carried[1][None, :]
        mixed_in = (jax.nn.gelu(branch.astype(jnp.float32)) * state_seq).astype(jnp.bfloat16)
        partial_value = jnp.dot(mixed_in, out_full, preferred_element_type=jnp.float32)
        mixed_sum = summed_on_arrival(partial_value.astype(jnp.bfloat16), "tp", 1)
        own_cols = (own_cols.astype(jnp.float32) + mixed_sum).astype(jnp.bfloat16)
        if tier_number + 1 < memory_path_matrix.shape[0]:
            full_rows = gather_rows(own_cols)
    floats = own_cols.astype(jnp.float32)
    full_width = floats.shape[1] * lax.axis_size("tp")
    square_sum = of_everyone(jnp.sum(floats * floats, axis=1), "tp")
    inv_rms = lax.rsqrt(square_sum / full_width + EPSILON)
    return (floats * inv_rms[:, None] * finishing_rms_gains[None, :]).astype(jnp.bfloat16)


def solution(mesh):
    return jax.shard_map(
        on_device,
        mesh=mesh,
        in_specs=(
            P(("grp", "sp"), "tp"),
            P(None, "sp", "tp"),
            P(None, "sp", "tp"),
            P(None, None, "tp"),
            P(None, "tp", None, None),
            P(None, "tp", None, None),
            P(None, "tp"),
            P(("grp", "sp")),
            P(("grp", "sp"), "tp"),
            P(None, "tp", "sp"),
            P(),
            P("tp"),
        ),
        out_specs=P(("grp", "sp"), "tp"),
        check_vma=False,
    )
```

profile of v0, /device:TPU:33, one launch (start us, length us, event | category | flops | bytes accessed | tf_op | source)
XLA Modules:
  0.0 602.2 jit_solution(12787368369105031495)
XLA Ops:
  6.6 0.8 slice_bitcast_fusion
  7.4 0.6 pad_maximum_fusion.10
  8.1 1.4 fusion.135
  9.6 1.1 copy.23
  10.7 1.3 broadcast_in_dim.6
  12.0 45.1 %all-to-all-start = ((bf16[8,384,256]{1,2,0:T(8,128)(2,1)}), bf16[8,384,256]{1,2,0:T(8,128)(2,1)S(1)}, u32[]{:S(2)}, u32[]{:S(2)}) async-start(bf16[8,384,256]{1,2,0:T(8,128)(2,1)} %broadcast_in_dim.6), calls=%async_computation | async-start | bytes 3145728 | tf_op jit(solution)/shard_map/all_to_all | solution.py:15
  57.1 0.6 pad_maximum_fusion.11
  59.1 18.7 %all-to-all-done = bf16[8,384,256]{1,2,0:T(8,128)(2,1)S(1)} async-done(((bf16[8,384,256]{1,2,0:T(8,128)(2,1)}), bf16[8,384,256]{1,2,0:T(8,128)(2,1)S(1)}, u32[]{:S(2)}, u32[]{:S(2)}) %all-to-all-start) | async-done | bytes 1572896 | tf_op jit(solution)/shard_map/all_to_all | solution.py:15
  78.6 72.2 %all-gather.11.cloned.1.call-done = bf16[2048,512]{1,0:T(8,128)(2,1)} async-done(((bf16[64,512]{1,0:T(8,128)(2,1)}), bf16[2048,512]{1,0:T(8,128)(2,1)}) %all-gather.11.cloned.1.call-update) | async-done | bytes 2097168 | tf_op jit(solution)/shard_map/all_gather | solution.py:32
  150.8 1.8 convolution_convert_fusion.4
  152.7 1.7 collective-permute-start
  154.4 0.7 collective-permute-done
  167.4 0.7 fusion.115
  168.1 0.7 pad_maximum_fusion.29
  168.8 0.6 pad_maximum_fusion.28
  169.5 0.7 fusion.112
  170.2 0.7 pad_maximum_fusion.25
  170.9 0.7 pad_maximum_fusion.24
  171.6 0.6 pad_maximum_fusion.21
  172.6 0.7 pad_maximum_fusion.13
  174.2 1.5 pad.227
  176.5 0.7 slice_add_fusion.5
  177.4 40.9 %all-gather.4 = f32[32,2,256]{2,1,0:T(2,128)S(1)} all-gather(f32[1,2,256]{2,1,0:T(2,128)S(1)} %maximum_bitcast_fusion), channel_id=2, replica_groups=mesh['grp'=2,'sp'=32,'tp'=8] {'sp'}, dimensions={0}, use_global_device_ids=true | all-gather | bytes 67584 | tf_op jit(solution)/shard_map/all_gather | solution.py:50
  218.4 59.8 %all-gather.15.cloned.1.call-done = bf16[1,256,2048]{1,2,0:T(8,128)(2,1)} async-done(((bf16[1,256,64]{1,2,0:T(8,128)(2,1)}), bf16[1,256,2048]{1,2,0:T(8,128)(2,1)}) %all-gather.15.cloned.1.call-update) | async-done | bytes 1048592 | tf_op jit(solution)/shard_map/all_gather | solution.py:100
  278.2 3.8 convolution_convert_fusion.1
  282.1 46.2 %all_to_all.26 = bf16[8,384,256]{2,1,0:T(8,128)(2,1)S(1)} all-to-all(bf16[8,384,256]{2,1,0:T(8,128)(2,1)S(1)} %bitcast.108), channel_id=1, replica_groups=mesh['grp'=2,'sp'=32,'tp'=8] {'tp'}, dimensions={0} | all-to-all | bytes 3145728 | tf_op jit(solution)/shard_map/all_to_all | solution.py:79
  328.6 0.7 copy-done.2
  329.5 1.3 broadcast_in_dim.7
  330.8 4.5 all-to-all-start.2
  335.9 20.1 %all-to-all-done.2 = bf16[8,384,256]{1,2,0:T(8,128)(2,1)S(1)} async-done(((bf16[8,384,256]{1,2,0:T(8,128)(2,1)}), bf16[8,384,256]{1,2,0:T(8,128)(2,1)S(1)}, u32[]{:S(2)}, u32[]{:S(2)}) %all-to-all-start.2) | async-done | bytes 1572896 | tf_op jit(solution)/shard_map/all_to_all | solution.py:15
  356.9 52.8 %all-gather.13.cloned.1.call-done = bf16[2048,512]{1,0:T(8,128)(2,1)} async-done(((bf16[64,512]{1,0:T(8,128)(2,1)}), bf16[2048,512]{1,0:T(8,128)(2,1)}) %all-gather.13.cloned.1.call-update) | async-done | bytes 2097168 | tf_op jit(solution)/shard_map/all_gather | solution.py:32
  409.7 1.8 convolution_convert_fusion.2
  411.6 1.5 collective-permute-start.1
  414.2 1.3 fusion.22
  415.9 0.8 slice.719
  416.7 1.0 multiply_add_fusion.2
  423.5 0.6 slice.763
  425.3 0.6 slice.765
  427.0 0.6 slice.732
  427.7 0.6 slice.767
  429.4 0.6 slice.726
  430.1 0.6 slice.769
  434.2 0.7 multiply_add_fusion.14
  435.0 0.7 fusion.120
  435.7 0.6 pad_maximum_fusion.31
  436.4 0.6 pad_maximum_fusion.30
  437.0 0.7 fusion.111
  437.8 0.6 pad_maximum_fusion.27
  438.4 0.7 pad_maximum_fusion.26
  439.1 0.7 fusion.109
  439.9 0.7 pad_maximum_fusion.23
  440.9 0.8 fusion.105
  441.7 0.6 pad_maximum_fusion.15
  442.4 0.6 pad_maximum_fusion.14
  443.3 1.6 pad.259
  445.6 0.7 slice_add_fusion.1
  446.4 1.7 pad.242
  448.1 0.7 slice_add_fusion
  448.8 41.6 %all-gather.5 = f32[32,2,256]{2,1,0:T(2,128)S(1)} all-gather(f32[1,2,256]{2,1,0:T(2,128)S(1)} %maximum_bitcast_fusion.1), channel_id=4, replica_groups=mesh['grp'=2,'sp'=32,'tp'=8] {'sp'}, dimensions={0}, use_global_device_ids=true | all-gather | bytes 67584 | tf_op jit(solution)/shard_map/all_gather | solution.py:50
  490.5 45.1 %all-gather.17.cloned.1.call-done = bf16[1,256,2048]{1,2,0:T(8,128)(2,1)} async-done(((bf16[1,256,64]{1,2,0:T(8,128)(2,1)}), bf16[1,256,2048]{1,2,0:T(8,128)(2,1)}) %all-gather.17.cloned.1.call-update) | async-done | bytes 1048592 | tf_op jit(solution)/shard_map/all_gather | solution.py:100
  535.7 3.9 convolution_convert_fusion
  539.7 46.7 %all_to_all.27 = bf16[8,384,256]{2,1,0:T(8,128)(2,1)S(1)} all-to-all(bf16[8,384,256]{2,1,0:T(8,128)(2,1)S(1)} %bitcast.109), channel_id=1, replica_groups=mesh['grp'=2,'sp'=32,'tp'=8] {'tp'}, dimensions={0} | all-to-all | bytes 3145728 | tf_op jit(solution)/shard_map/all_to_all | solution.py:79
  586.7 8.1 %all_to_all.28 = f32[8,1,384]{2,1,0:T(1,128)S(1)} all-to-all(f32[8,1,384]{2,1,0:T(1,128)S(1)} %broadcast_in_dim.8), channel_id=1, replica_groups=mesh['grp'=2,'sp'=32,'tp'=8] {'tp'}, dimensions={0} | all-to-all | bytes 24576 | tf_op jit(solution)/shard_map/all_to_all | solution.py:15
  594.9 0.8 fusion.36
  (356 shorter events, 34.4 us)
Async XLA Ops:
  6.5 144.2 %all-gather.11.cloned.1.call-start = ((), (), s32[]{:S(2)}) async-start(), calls=%async_computation.5 | async-start | bytes 2162688 | tf_op jit(solution)/shard_map/all_gather | solution.py:32
  8.1 270.1 %all-gather.15.cloned.1.call-start = ((), (), s32[]{:S(2)}) async-start(), calls=%async_computation.7 | async-start | bytes 1081344 | tf_op jit(solution)/shard_map/all_gather | solution.py:100
  12.0 45.8 %copy-start.28 = (f32[2,256]{1,0:T(2,128)S(1)}, f32[2,256]{1,0:T(2,128)}, u32[]{:S(2)}) copy-start(f32[2,256]{1,0:T(2,128)} %param.22) | copy-start | bytes 6148
  12.0 46.4 %copy-start.11 = (bf16[2,4,256]{2,1,0:T(4,128)(2,1)S(1)}, bf16[2,4,256]{2,1,0:T(4,128)(2,1)}, u32[]{:S(2)}) copy-start(bf16[2,4,256]{2,1,0:T(4,128)(2,1)} %param.19) | copy-start | bytes 12292
  12.0 47.0 %copy-start.10 = (f32[2,2048]{1,0:T(2,128)S(1)}, f32[2,2048]{1,0:T(2,128)}, u32[]{:S(2)}) copy-start(f32[2,2048]{1,0:T(2,128)} %param.26) | copy-start | bytes 49156
  12.0 65.7 %all-to-all-start = ((bf16[8,384,256]{1,2,0:T(8,128)(2,1)}), bf16[8,384,256]{1,2,0:T(8,128)(2,1)S(1)}, u32[]{:S(2)}, u32[]{:S(2)}) async-start(bf16[8,384,256]{1,2,0:T(8,128)(2,1)} %broadcast_in_dim.6), calls=%async_computation | async-start | bytes 3145728 | tf_op jit(solution)/shard_map/all_to_all | solution.py:15
  57.1 352.6 %all-gather.13.cloned.1.call-start = ((), (), s32[]{:S(2)}) async-start(), calls=%async_computation.6 | async-start | bytes 2162688 | tf_op jit(solution)/shard_map/all_gather | solution.py:32
  78.6 76.7 %copy-start.31 = (f32[384,256]{1,0:T(8,128)S(1)}, f32[384,256]{1,0:T(8,128)}, u32[]{:S(2)}) copy-start(f32[384,256]{1,0:T(8,128)} %param.24) | copy-start | bytes 1179652
  78.6 76.7 %copy-start.33 = (bf16[2,1,256,256]{3,2,1,0:T(8,128)(2,1)S(1)}, bf16[2,1,256,256]{3,2,1,0:T(8,128)(2,1)}, u32[]{:S(2)}) copy-start(bf16[2,1,256,256]{3,2,1,0:T(8,128)(2,1)} %param.20) | copy-start | bytes 786436
  78.6 76.7 %copy-start.36 = (f32[384]{0:T(512)S(1)}, f32[384]{0:T(512)}, u32[]{:S(2)}) copy-start(f32[384]{0:T(512)} %param.23) | copy-start | bytes 4612
  152.6 3.0 copy-start.35
  152.7 2.5 collective-permute-start
  156.1 11.2 %copy-start = (f32[384,256]{1,0:T(8,128)}, f32[384,256]{1,0:T(8,128)S(1)}, u32[]{:S(2)}) copy-start(f32[384,256]{1,0:T(8,128)S(1)} %fusion.25) | copy-start | bytes 1179652
  165.6 6.7 %copy-start.26 = (f32[1,256]{1,0:T(1,128)S(1)}, f32[1,256]{1,0:T(1,128)}, u32[]{:S(2)}) copy-start(f32[1,256]{1,0:T(1,128)} %slice.803) | copy-start | bytes 3076
  165.6 6.8 %copy-start.24 = (f32[1,256]{1,0:T(1,128)S(1)}, f32[1,256]{1,0:T(1,128)}, u32[]{:S(2)}) copy-start(f32[1,256]{1,0:T(1,128)} %slice.828) | copy-start | bytes 3076
  165.6 6.9 %copy-start.22 = (f32[1,256]{1,0:T(1,128)S(1)}, f32[1,256]{1,0:T(1,128)}, u32[]{:S(2)}) copy-start(f32[1,256]{1,0:T(1,128)} %slice.802) | copy-start | bytes 3076
  172.4 1.6 copy-start.20
  174.0 1.8 copy-start.18
  175.7 0.6 copy-start.16
  175.9 1.4 slice-start
  176.5 101.7 %copy-start.5 = (f32[384,256]{1,0:T(8,128)}, f32[384,256]{1,0:T(8,128)S(1)}, u32[]{:S(2)}) copy-start(f32[384,256]{1,0:T(8,128)S(1)} %pad.226) | copy-start | bytes 1179652
  177.2 101.0 %copy-start.6 = (f32[384,256]{1,0:T(8,128)}, f32[384,256]{1,0:T(8,128)S(1)}, u32[]{:S(2)}) copy-start(f32[384,256]{1,0:T(8,128)S(1)} %pad.211) | copy-start | bytes 1179652
  328.3 0.9 copy-start.2
  330.8 25.2 %all-to-all-start.2 = ((bf16[8,384,256]{1,2,0:T(8,128)(2,1)}), bf16[8,384,256]{1,2,0:T(8,128)(2,1)S(1)}, u32[]{:S(2)}, u32[]{:S(2)}) async-start(bf16[8,384,256]{1,2,0:T(8,128)(2,1)} %broadcast_in_dim.7), calls=%async_computation.2 | async-start | bytes 3145728 | tf_op jit(solution)/shard_map/all_to_all | solution.py:15
  335.3 200.3 %all-gather.17.cloned.1.call-start = ((), (), s32[]{:S(2)}) async-start(), calls=%async_computation.8 | async-start | bytes 1081344 | tf_op jit(solution)/shard_map/all_gather | solution.py:100
  356.8 56.7 %copy-start.12 = (f32[1,1,256]{2,1,0:T(1,128)S(1)}, f32[1,1,256]{2,1,0:T(1,128)}, u32[]{:S(2)}) copy-start(f32[1,1,256]{2,1,0:T(1,128)} %get-tuple-element.193) | copy-start | bytes 3076
  356.9 56.7 %copy-start.13 = (f32[1,1,256]{2,1,0:T(1,128)S(1)}, f32[1,1,256]{2,1,0:T(1,128)}, u32[]{:S(2)}) copy-start(f32[1,1,256]{2,1,0:T(1,128)} %get-tuple-element.194) | copy-start | bytes 3076
  356.9 56.7 %copy-start.14 = (f32[1,1,256]{2,1,0:T(1,128)S(1)}, f32[1,1,256]{2,1,0:T(1,128)}, u32[]{:S(2)}) copy-start(f32[1,1,256]{2,1,0:T(1,128)} %get-tuple-element.199) | copy-start | bytes 3076
  356.9 56.7 %copy-start.15 = (f32[1,1,256]{2,1,0:T(1,128)S(1)}, f32[1,1,256]{2,1,0:T(1,128)}, u32[]{:S(2)}) copy-start(f32[1,1,256]{2,1,0:T(1,128)} %get-tuple-element.200) | copy-start | bytes 3076
  356.9 56.9 %copy-start.30 = (f32[1,256]{1,0:T(1,128)S(1)}, f32[1,256]{1,0:T(1,128)}, u32[]{:S(2)}) copy-start(f32[1,256]{1,0:T(1,128)} %get-tuple-element.209) | copy-start | bytes 3076
  356.9 56.9 %copy-start.32 = (f32[384,256]{1,0:T(8,128)S(1)}, f32[384,256]{1,0:T(8,128)}, u32[]{:S(2)}) copy-start(f32[384,256]{1,0:T(8,128)} %param.24) | copy-start | bytes 1179652
  356.9 56.9 %copy-start.34 = (bf16[2,1,256,256]{3,2,1,0:T(8,128)(2,1)S(1)}, bf16[2,1,256,256]{3,2,1,0:T(8,128)(2,1)}, u32[]{:S(2)}) copy-start(bf16[2,1,256,256]{3,2,1,0:T(8,128)(2,1)} %param.20) | copy-start | bytes 786436
  356.9 56.9 %copy-start.37 = (f32[384]{0:T(512)S(1)}, f32[384]{0:T(512)}, u32[]{:S(2)}) copy-start(f32[384]{0:T(512)} %param.23) | copy-start | bytes 4612
  411.6 2.0 collective-permute-start.1
  415.5 18.7 %copy-start.1 = (f32[384,256]{1,0:T(8,128)}, f32[384,256]{1,0:T(8,128)S(1)}, u32[]{:S(2)}) copy-start(f32[384,256]{1,0:T(8,128)S(1)} %fusion.22) | copy-start | bytes 1179652
  432.5 8.1 %copy-start.27 = (f32[1,256]{1,0:T(1,128)S(1)}, f32[1,256]{1,0:T(1,128)}, u32[]{:S(2)}) copy-start(f32[1,256]{1,0:T(1,128)} %slice.862) | copy-start | bytes 3076
  432.5 8.2 %copy-start.8 = (f32[23,256]{1,0:T(8,128)S(1)}, f32[23,256]{1,0:T(8,128)}, u32[]{:S(2)}) copy-start(f32[23,256]{1,0:T(8,128)} %slice.732) | copy-start | bytes 70660
  432.5 8.2 %copy-start.9 = (f32[23,256]{1,0:T(8,128)S(1)}, f32[23,256]{1,0:T(8,128)}, u32[]{:S(2)}) copy-start(f32[23,256]{1,0:T(8,128)} %slice.767) | copy-start | bytes 70660
  432.5 8.2 %copy-start.25 = (f32[1,256]{1,0:T(1,128)S(1)}, f32[1,256]{1,0:T(1,128)}, u32[]{:S(2)}) copy-start(f32[1,256]{1,0:T(1,128)} %slice.887) | copy-start | bytes 3076
  432.5 8.3 %copy-start.23 = (f32[1,256]{1,0:T(1,128)S(1)}, f32[1,256]{1,0:T(1,128)}, u32[]{:S(2)}) copy-start(f32[1,256]{1,0:T(1,128)} %slice.861) | copy-start | bytes 3076
  432.5 8.4 %copy-start.7 = (f32[47,256]{1,0:T(8,128)S(1)}, f32[47,256]{1,0:T(8,128)}, u32[]{:S(2)}) copy-start(f32[47,256]{1,0:T(8,128)} %slice.769) | copy-start | bytes 144388
  440.7 2.4 copy-start.21
  443.1 1.8 copy-start.19
  444.9 0.7 copy-start.17
  445.0 1.4 slice-start.1
  445.6 90.0 %copy-start.3 = (f32[384,256]{1,0:T(8,128)}, f32[384,256]{1,0:T(8,128)S(1)}, u32[]{:S(2)}) copy-start(f32[384,256]{1,0:T(8,128)S(1)} %pad.258) | copy-start | bytes 1179652
  446.4 89.3 %copy-start.4 = (f32[384,256]{1,0:T(8,128)}, f32[384,256]{1,0:T(8,128)S(1)}, u32[]{:S(2)}) copy-start(f32[384,256]{1,0:T(8,128)S(1)} %pad.243) | copy-start | bytes 1179652
  586.3 8.5 %copy-start.29 = (f32[256]{0:T(256)S(1)}, f32[256]{0:T(256)}, u32[]{:S(2)}) copy-start(f32[256]{0:T(256)} %param.27) | copy-start | bytes 3076
Sparse Core Ops, SparseCore 0:
  9.4 141.3 all-gather.10
  152.9 125.2 all-gather.14
  280.3 129.3 all-gather.12
  411.6 123.9 all-gather.16
where the time goes:
time: 604 us; the launch traced here: 602 us
  waiting for transfers between devices  271 us (45%)
  blocking collectives  183 us (30%)
  starting transfers between devices  52.9 us (9%)
  local copies, waits for them, and re-layouts  42.2 us (7%)
  other arithmetic  24.4 us (4%)
  between operations  14.8 us (2%)
  matrix products  13.7 us (2%)
    all_gather x2, waiting for transfers between devices, in_one_piece(): whole = lax.all_gather(both, axis, axis=dim, tiled=True)  125 us
    all_gather x2, waiting for transfers between devices, fetch_layer(): lax.all_gather(exit_projector_matrix[tier_number], 'sp', axis=1, tiled=True)  105 us
    all_to_all x2, blocking collectives, summed_on_arrival(): lax.all_to_all(tiles, axis, split_axis=0, concat_axis=0, tiled=True)  92.9 us
    all_gather x2, blocking collectives, gathered_once(): both, at, found = (lax.all_gather(jnp.concatenate(lines), axis), 0, {})  82.5 us
    all_to_all x2, starting transfers between devices, sent_to_all(): return lax.all_to_all(copies, axis, split_axis=0, concat_axis=0, tiled=True)  49.6 us
    all_to_all x2, waiting for transfers between devices, sent_to_all(): return lax.all_to_all(copies, axis, split_axis=0, concat_axis=0, tiled=True)  38.8 us
    slice x114, local copies, waits for them, and re-layouts, on_device(): lax.associative_scan(combine_pairs, (keep_rate, driven), axis=0)  28.4 us
  transfers between devices with their start and end apart: 8, of which 8 were waited for; matrix products, arithmetic and copies ran while one was open for 12% of the time, Pallas kernels for 0%

commit v1 on v0

v1 whole, which is shorter than its diff:
```python
import functools

import jax
import jax.numpy as jnp
from jax import lax
from jax.experimental import pallas as pl
from jax.experimental.pallas import tpu as pltpu
from jax.sharding import PartitionSpec as P

EPSILON = 1e-06
SQUASH_POWER = 8.0
SEGS = 8
MESH = pl.DeviceIdType.MESH
F32 = jnp.float32
BF16 = jnp.bfloat16
NT = (((1,), (1,)), ((), ()))


def one_minus_exp(y):
    series = 1.0 + y * (1.0 / 8.0)
    for n in (7, 6, 5, 4, 3, 2):
        series = 1.0 + y * (1.0 / n) * series
    return jnp.where(y > -0.35, -y * series, 1.0 - jnp.exp(y))


def softplus(v):
    u = jnp.exp(-jnp.abs(v))
    s = u / (2.0 + u)
    s2 = s * s
    acc = jnp.full_like(s, 1.0 / 17.0)
    for n in (15, 13, 11, 9, 7, 5, 3, 1):
        acc = acc * s2 + 1.0 / n
    return jnp.maximum(v, 0.0) + 2.0 * s * acc


def gelu(x):
    inner = 0.7978845608028654 * (x + 0.044715 * (x * x * x))
    return 0.5 * x * (1.0 + jnp.tanh(inner))


def kernel(
    n_sp,
    n_x,
    x_hbm,
    wm_hbm,
    wp_hbm,
    ex_hbm,
    rv_hbm,
    iv_hbm,
    spike_hbm,
    filt_ref,
    forget_ref,
    tm_ref,
    gain_ref,
    fin_ref,
    out_ref,
    xin,
    exin,
    rv,
    iv,
    spike_in,
    spk,
    tmc,
    xf,
    w,
    nrm,
    rec,
    br,
    kp,
    dr,
    pp,
    own32,
    psnd,
    prcv,
    rsnd,
    rrcv,
    hsnd,
    hrcv,
    csnd,
    crcv,
    nsnd,
    nrcv,
    lsem,
    z_s,
    z_r,
    ag_s,
    ag_r,
    ad_s,
    ad_r,
    rs_s,
    rs_r,
    rd_s,
    rd_r,
    h_s,
    h_r,
    c_s,
    c_r,
    n_s,
    n_r,
):
    layers = wm_hbm.shape[0]
    rows, cols = x_hbm.shape
    half = rows // 2
    steps = rows // SEGS
    chunk = wm_hbm.shape[1]
    n_tp = 2 * n_x
    z = lax.axis_index("sp")
    me = lax.axis_index("tp")
    x = me // 2
    c = lax.rem(me, 2)
    other = 1 - c
    z_up, z_dn = lax.rem(z + 1, n_sp), lax.rem(z + n_sp - 1, n_sp)
    x_rt, x_lf, x_far = lax.rem(x + 1, n_x), lax.rem(x + n_x - 1, n_x), lax.rem(x + 2, n_x)
    mate = {"tp": 2 * x + other}
    right, left = {"tp": 2 * x_rt + c}, {"tp": 2 * x_lf + c}
    up, down = {"sp": z_up}, {"sp": z_dn}

    def remote(src, dst, ssem, rsem, dev):
        return pltpu.make_async_remote_copy(
            src_ref=src, dst_ref=dst, send_sem=ssem, recv_sem=rsem, device_id=dev, device_id_type=MESH
        )

    own_rows = pl.ds(pl.multiple_of(z * chunk, chunk), chunk)
    local = [
        pltpu.make_async_copy(x_hbm, xin, lsem.at[0]),
        pltpu.make_async_copy(ex_hbm, exin, lsem.at[1]),
        pltpu.make_async_copy(rv_hbm, rv, lsem.at[2]),
        pltpu.make_async_copy(iv_hbm, iv, lsem.at[3]),
        pltpu.make_async_copy(spike_hbm, spike_in, lsem.at[4]),
    ]
    for l in range(layers):
        local.append(pltpu.make_async_copy(wp_hbm.at[l], w.at[l, 0, own_rows, :], lsem.at[5 + 2 * l]))
        local.append(pltpu.make_async_copy(wm_hbm.at[l], w.at[l, 1, own_rows, :], lsem.at[6 + 2 * l]))
    for copy in local:
        copy.start()

    barrier = pltpu.get_barrier_semaphore()
    for dev in (up, down):
        pl.semaphore_signal(barrier, inc=1, device_id=dev, device_id_type=MESH)
    for k in range(1, n_tp):
        pl.semaphore_signal(
            barrier, inc=1, device_id={"tp": lax.rem(me + k, n_tp)}, device_id_type=MESH
        )
    pl.semaphore_wait(barrier, n_tp + 1)

    last_up, last_dn = n_sp // 2, n_sp - 1 - n_sp // 2

    def z_copy(l, m, d, s):
        src = lax.rem(z - s + n_sp, n_sp) if d == 0 else lax.rem(z + s, n_sp)
        ref = w.at[l, m, pl.ds(pl.multiple_of(src * chunk, chunk), chunk), :]
        return remote(ref, ref, z_s.at[l, m, d, s], z_r.at[l, m, d, s], up if d == 0 else down)

    def z_land(l, m, d, s):
        src = lax.rem(z - s - 1 + n_sp, n_sp) if d == 0 else lax.rem(z + s + 1, n_sp)
        ref = w.at[l, m, pl.ds(pl.multiple_of(src * chunk, chunk), chunk), :]
        return remote(ref, ref, z_s.at[l, m, d, s], z_r.at[l, m, d, s], up if d == 0 else down)

    def ring_start(l, m):
        z_copy(l, m, 0, 0).start()
        z_copy(l, m, 1, 0).start()

    def ring_steps(l, first, last):
        both = min(last, last_dn - 1)

        def one(s, _):
            for m in range(3):
                for d in range(2):
                    z_land(l, m, d, s).wait_recv()
                    z_copy(l, m, d, s + 1).start()
            return 0

        if both > first:
            lax.fori_loop(first, both, one, 0)
        for s in range(max(first, both), last):
            for m in range(3):
                if s < last_up:
                    z_land(l, m, 0, s).wait_recv()
                    if s + 1 < last_up:
                        z_copy(l, m, 0, s + 1).start()
                if s < last_dn:
                    z_land(l, m, 1, s).wait_recv()
                    if s + 1 < last_dn:
                        z_copy(l, m, 1, s + 1).start()

    for i in (5, 6, 1):
        local[i].wait()
    ring_start(0, 0)
    ring_start(0, 1)
    for l in range(layers):
        w[l, 2, own_rows, :] = exin[l].astype(F32).T.astype(BF16)
    ring_start(0, 2)

    row_p = lax.broadcasted_iota(jnp.int32, (rows, rows), 0)
    row_r = lax.broadcasted_iota(jnp.int32, (rows, rows), 1)
    onehot = row_r == (row_p & (SEGS - 1)) * steps + (row_p >> 3)
    local[0].wait()
    xf[0, me] = jnp.dot(onehot.astype(BF16), xin[...], preferred_element_type=F32).astype(BF16)

    top, bottom = pl.ds(0, half), pl.ds(half, half)

    def ag_copy(l, i):
        block, part, dev = (
            (2 * x + c, top, right),
            (2 * x + c, bottom, right),
            (2 * x_lf + c, top, right),
            (2 * x + c, bottom, left),
            (2 * x + c, top, left),
            (2 * x_rt + c, bottom, left),
        )[i]
        ref = xf.at[l, block, part, :]
        return remote(ref, ref, ag_s.at[l, i], ag_r.at[l, i], dev)

    def ag_land(l, i):
        block, part = (
            (2 * x_lf + c, top),
            (2 * x_lf + c, bottom),
            (2 * x_far + c, top),
            (2 * x_rt + c, bottom),
            (2 * x_rt + c, top),
            (2 * x_far + c, bottom),
        )[i]
        ref = xf.at[l, block, part, :]
        return remote(ref, ref, ag_s.at[l, i], ag_r.at[l, i], right)

    def ad_copy(l, i):
        ref = xf.at[l, 2 * (x, x_lf, x_rt, x_far)[i] + c]
        return remote(ref, ref, ad_s.at[l, i], ad_r.at[l, i], mate)

    def ad_land(l, i):
        ref = xf.at[l, 2 * (x, x_lf, x_rt, x_far)[i] + other]
        return remote(ref, ref, ad_s.at[l, i], ad_r.at[l, i], mate)

    def ag_start(l):
        for i in (0, 3, 1, 4):
            ag_copy(l, i).start()
        ad_copy(l, 0).start()

    def ag_forward(l):
        ag_land(l, 0).wait_recv()
        ag_copy(l, 2).start()
        ag_land(l, 3).wait_recv()
        ag_copy(l, 5).start()

    def ag_near(l):
        ag_land(l, 1).wait_recv()
        ad_copy(l, 1).start()
        ag_land(l, 4).wait_recv()
        ad_copy(l, 2).start()

    def ag_far(l):
        ag_land(l, 2).wait_recv()
        ag_land(l, 5).wait_recv()
        ad_copy(l, 3).start()
        for i in range(4):
            ad_land(l, i).wait_recv()

    def normalize(l):
        size = 32

        def one(i, _):
            part = pl.ds(pl.multiple_of(i * size, size), size)
            total = jnp.zeros((size, cols), F32)
            for b in range(n_tp):
                v = xf[l, b, part, :].astype(F32)
                total = total + v * v
            inv = lax.rsqrt(jnp.sum(total, axis=1, keepdims=True) / (n_tp * cols) + EPSILON)
            for b in range(n_tp):
                g = gain_ref[l : l + 1, b * cols : (b + 1) * cols]
                nrm[part, b * cols : (b + 1) * cols] = (xf[l, b, part, :].astype(F32) * inv * g).astype(BF16)
            return 0

        lax.fori_loop(0, rows // size, one, 0)

    def recurrent(l):
        rec[pl.ds(24, rows), :] = (
            jnp.dot(nrm[...], w[l, 0], preferred_element_type=F32).astype(BF16).astype(F32)
        )
        for j in range(3):
            at = 24 + rows - 24 + 8 * j + 7
            hsnd[l, j : j + 1, :] = rec[at : at + 1, :]
        h_copy = remote(hsnd.at[l], hrcv.at[l], h_s.at[l], h_r.at[l], up)

        @pl.when(z < n_sp - 1)
        def _():
            h_copy.start()

        @pl.when(z == 0)
        def _():
            hrcv[l] = jnp.zeros((8, cols), F32)

        @pl.when(z > 0)
        def _():
            h_copy.wait_recv()

        first = lax.broadcasted_iota(jnp.int32, (8, cols), 0) == 0
        for j in range(3):
            tail = rec[rows + 8 * j : rows + 8 * j + 8, :]
            rec[8 * j : 8 * j + 8, :] = jnp.where(
                first, jnp.broadcast_to(hrcv[l, j : j + 1, :], (8, cols)), pltpu.roll(tail, 1, 0)
            )

        @pl.when(z < n_sp - 1)
        def _():
            h_copy.wait_send()

    def gates(l):
        size = 64
        rate = softplus(-forget_ref[l : l + 1, :]) * -SQUASH_POWER
        f = filt_ref[l].astype(F32)

        def one(i, _):
            base = pl.multiple_of(i * size, size)
            conv = jnp.zeros((size, cols), F32)
            for k in range(4):
                conv = conv + rec[pl.ds(pl.multiple_of(base + 8 * k, 8), size), :] * f[k : k + 1, :]
            conv = conv.astype(BF16)
            reset = jax.nn.sigmoid(jnp.dot(conv, rv[l, 0], preferred_element_type=F32))
            inject = jax.nn.sigmoid(jnp.dot(conv, iv[l, 0], preferred_element_type=F32))
            part = pl.ds(base, size)
            tmb = jnp.concatenate([tmc[part, :]] * (cols // 128), axis=1)
            log_keep = reset * rate * tmb + spk[part, :]
            kp[part, :] = jnp.exp(log_keep)
            dr[part, :] = inject * conv.astype(F32) * jnp.sqrt(one_minus_exp(2.0 * log_keep))
            return 0

        lax.fori_loop(0, rows // size, one, 0)

    def scan(l):
        def one(i, carry):
            s, p = carry
            part = pl.ds(pl.multiple_of(i * SEGS, SEGS), SEGS)
            k = kp[part, :]
            s = k * s + dr[part, :]
            p = p * k
            dr[part, :] = s
            pp[part, :] = p
            return s, p

        s, p = lax.fori_loop(
            0, steps, one, (jnp.zeros((SEGS, cols), F32), jnp.ones((SEGS, cols), F32)), unroll=8
        )
        state, prod = jnp.zeros((1, cols), F32), jnp.ones((1, cols), F32)
        states, prods = [], []
        for j in range(SEGS):
            states.append(state)
            prods.append(prod)
            state = p[j : j + 1] * state + s[j : j + 1]
            prod = prod * p[j : j + 1]
        csnd[l, 0:1, :] = prod
        csnd[l, 1:2, :] = state
        return jnp.concatenate(states, axis=0), jnp.concatenate(prods, axis=0)

    def c_copy(l, target):
        return remote(csnd.at[l], crcv.at[l, z], c_s.at[l, target], c_r.at[l, z], {"sp": target})

    def carry_send(l):
        def one(n, _):
            for k in (n_sp // 2 - n, n_sp // 2 + 1 + n):
                target = z + k

                @pl.when(target < n_sp)
                def _():
                    c_copy(l, target).start()

            return 0

        lax.fori_loop(0, n_sp // 2, one, 0)

    def carry_wait(l):
        def one(n, carry):
            state, prod = carry
            j = z - 1 - n
            remote(csnd.at[l], crcv.at[l, j], c_s.at[l, j], c_r.at[l, j], {"sp": j}).wait_recv()
            state = state + prod * crcv[l, j, 1:2, :]
            prod = prod * crcv[l, j, 0:1, :]
            return state, prod

        return lax.fori_loop(0, z, one, (jnp.zeros((1, cols), F32), jnp.ones((1, cols), F32)))[0]

    def carry_drain(l):
        def one(target, _):
            c_copy(l, target).wait_send()
            return 0

        lax.fori_loop(z + 1, n_sp, one, 0)

    def branch(l):
        br[...] = gelu(jnp.dot(nrm[...], w[l, 1], preferred_element_type=F32).astype(BF16).astype(F32))

    def mix(carry):
        def one(i, _):
            part = pl.ds(pl.multiple_of(i * SEGS, SEGS), SEGS)
            br[part, :] = br[part, :] * (dr[part, :] + pp[part, :] * carry)
            return 0

        lax.fori_loop(0, steps, one, 0, unroll=8)

    def product(l, mixed, block):
        e = w[l, 2, pl.ds(pl.multiple_of(block * cols, cols), cols), :]
        return lax.dot_general(mixed, e, NT, preferred_element_type=F32)

    order = (x_far, x_rt, x_lf, x)

    def rd(l, i):
        return remote(psnd.at[i], prcv.at[l, i], rd_s.at[l, i], rd_r.at[l, i], mate)

    def rs(l, i):
        return remote(rsnd.at[i], rrcv.at[l, i], rs_s.at[l, i], rs_r.at[l, i], right if i < 3 else left)

    def rs_products(l):
        mixed = br[...].astype(BF16)
        for i in range(4):
            psnd[i] = product(l, mixed, 2 * order[i] + other).astype(BF16)
            rd(l, i).start()
        for i in range(4):
            own32[i] = product(l, mixed, 2 * order[i] + c)

    def pair(l, i, part):
        return own32[i, part, :] + prcv[l, i, part, :].astype(F32)

    def rs_first(l):
        rd(l, 0).wait_recv()
        rsnd[0] = pair(l, 0, top).astype(BF16)
        rs(l, 0).start()
        rsnd[3] = pair(l, 0, bottom).astype(BF16)
        rs(l, 3).start()
        rd(l, 1).wait_recv()
        rsnd[1] = pair(l, 1, bottom).astype(BF16)
        rs(l, 1).start()
        rd(l, 2).wait_recv()
        rsnd[4] = pair(l, 2, top).astype(BF16)
        rs(l, 4).start()

    def rs_second(l):
        rs(l, 0).wait_recv()
        rsnd[2] = (pair(l, 1, top) + rrcv[l, 0].astype(F32)).astype(BF16)
        rs(l, 2).start()
        rs(l, 3).wait_recv()
        rsnd[5] = (pair(l, 2, bottom) + rrcv[l, 3].astype(F32)).astype(BF16)
        rs(l, 5).start()

    def rs_last(l):
        rd(l, 3).wait_recv()
        parts = []
        for i in (1, 4, 2, 5):
            rs(l, i).wait_recv()
        for part, (a, b) in ((top, (2, 4)), (bottom, (1, 5))):
            total = pair(l, 3, part) + rrcv[l, a].astype(F32) + rrcv[l, b].astype(F32)
            parts.append((xf[l, me, part, :].astype(F32) + total).astype(BF16))
        for i in range(4):
            rd(l, i).wait_send()
        for i in range(6):
            rs(l, i).wait_send()
        return parts

    ag_start(0)
    ring_steps(0, 0, 2)
    ag_forward(0)
    ring_steps(0, 2, 4)
    ag_near(0)
    ring_steps(0, 4, 6)
    ag_far(0)
    tm_b = jnp.broadcast_to(tm_ref[...], (rows, rows))
    tmc[...] = jnp.broadcast_to(
        jnp.sum(jnp.where(onehot, tm_b, 0.0), axis=1, keepdims=True), tmc.shape
    )
    ring_steps(0, 6, 7)
    local[4].wait()
    spk[...] = jnp.dot(
        onehot.astype(F32), spike_in[...], preferred_element_type=F32, precision=lax.Precision.HIGHEST
    )
    ring_steps(0, 7, 8)
    normalize(0)
    ring_steps(0, 8, last_up)
    for i in (2, 3):
        local[i].wait()
    for l in range(1, layers):
        local[5 + 2 * l].wait()
        local[6 + 2 * l].wait()
        for m in range(3):
            ring_start(l, m)

    parts = None
    for l in range(layers):
        more = l + 1 < layers
        if l > 0:
            ag_start(l)
            ag_forward(l)
            ring_steps(l, 12, 13)
            ag_near(l)
            ring_steps(l, 13, 14)
            ag_far(l)
            normalize(l)
            ring_steps(l, 14, last_up)
        recurrent(l)
        gates(l)
        seg_state, seg_prod = scan(l)
        carry_send(l)
        branch(l)
        if more:
            ring_steps(l + 1, 0, 5)
        carry = carry_wait(l)
        mix(seg_state + seg_prod * carry)
        carry_drain(l)
        rs_products(l)
        rs_first(l)
        if more:
            ring_steps(l + 1, 5, 7)
        rs_second(l)
        if more:
            ring_steps(l + 1, 7, 9)
        parts = rs_last(l)
        if more:
            xf[l + 1, me, top, :] = parts[0]
            xf[l + 1, me, bottom, :] = parts[1]
            ring_steps(l + 1, 9, 12)

    final = jnp.concatenate(parts, axis=0).astype(F32)
    squares = jnp.sum(final * final, axis=1, keepdims=True)
    wide = jnp.transpose(jnp.broadcast_to(squares, (rows, 128)))
    nsnd[...] = wide[0:8, :]

    def n_copy(k):
        return remote(nsnd, nrcv.at[me], n_s.at[k], n_r.at[k], {"tp": lax.rem(me + k, n_tp)})

    for k in range(1, n_tp):
        n_copy(k).start()
    total = nsnd[...]
    for k in range(1, n_tp):
        n_copy(k).wait_recv()
    for k in range(1, n_tp):
        total = total + nrcv[lax.rem(me + k, n_tp)]
    inv = lax.rsqrt(total / (n_tp * cols) + EPSILON)
    inv = jnp.transpose(jnp.broadcast_to(inv[0:1, :], (128, rows)))
    inv = jnp.concatenate([inv] * (cols // 128), axis=1)
    result = (final * inv * fin_ref[...]).astype(BF16)
    back = row_p == (row_r & (SEGS - 1)) * steps + (row_r >> 3)
    out_ref[...] = jnp.dot(back.astype(BF16), result, preferred_element_type=F32).astype(BF16)

    for k in range(1, n_tp):
        n_copy(k).wait_send()
    for l in range(layers):
        for i in range(6):
            ag_copy(l, i).wait_send()
        for i in range(4):
            ad_copy(l, i).wait_send()
        for m in range(3):
            for d, last in ((0, last_up), (1, last_dn)):

                def one(s, _, l=l, m=m, d=d):
                    z_copy(l, m, d, s).wait_send()
                    return 0

                lax.fori_loop(0, last, one, 0)


def on_device(
    n_sp,
    n_tp,
    starting_stream,
    multiplier_matrix,
    memory_path_matrix,
    filter_coefficients,
    memory_valve_matrix,
    entry_valve_matrix,
    forgetting_parameters,
    timestep_forgetting_multiplier,
    spike_extra,
    exit_projector_matrix,
    prelude_rms_gains,
    finishing_rms_gains,
):
    rows, cols = starting_stream.shape
    layers, chunk, width = memory_path_matrix.shape
    half = rows // 2
    full = n_sp * chunk
    n_x = n_tp // 2
    hbm = pl.BlockSpec(memory_space=pl.ANY)
    vmem = pl.BlockSpec(memory_space=pltpu.VMEM)
    dma = pltpu.SemaphoreType.DMA
    scratch = [
        pltpu.VMEM((rows, cols), BF16),
        pltpu.VMEM(exit_projector_matrix.shape, BF16),
        pltpu.VMEM(memory_valve_matrix.shape, BF16),
        pltpu.VMEM(entry_valve_matrix.shape, BF16),
        pltpu.VMEM((rows, cols), F32),
        pltpu.VMEM((rows, cols), F32),
        pltpu.VMEM((rows, 128), F32),
        pltpu.VMEM((layers, n_tp, rows, cols), BF16),
        pltpu.VMEM((layers, 3, full, cols), BF16),
        pltpu.VMEM((rows, full), BF16),
        pltpu.VMEM((rows + 24, cols), F32),
        pltpu.VMEM((rows, cols), F32),
        pltpu.VMEM((rows, cols), F32),
        pltpu.VMEM((rows, cols), F32),
        pltpu.VMEM((rows, cols), F32),
        pltpu.VMEM((4, rows, cols), F32),
        pltpu.VMEM((4, rows, cols), BF16),
        pltpu.VMEM((layers, 4, rows, cols), BF16),
        pltpu.VMEM((6, half, cols), BF16),
        pltpu.VMEM((layers, 6, half, cols), BF16),
        pltpu.VMEM((layers, 8, cols), F32),
        pltpu.VMEM((layers, 8, cols), F32),
        pltpu.VMEM((layers, 2, cols), F32),
        pltpu.VMEM((layers, n_sp, 2, cols), F32),
        pltpu.VMEM((8, rows), F32),
        pltpu.VMEM((n_tp, 8, rows), F32),
        dma((9,)),
        dma((layers, 3, 2, n_sp // 2)),
        dma((layers, 3, 2, n_sp // 2)),
        dma((layers, 6)),
        dma((layers, 6)),
        dma((layers, 4)),
        dma((layers, 4)),
        dma((layers, 6)),
        dma((layers, 6)),
        dma((layers, 4)),
        dma((layers, 4)),
        dma((layers,)),
        dma((layers,)),
        dma((layers, n_sp)),
        dma((layers, n_sp)),
        dma((n_tp,)),
        dma((n_tp,)),
    ]
    return pl.pallas_call(
        functools.partial(kernel, n_sp, n_x),
        out_shape=jax.ShapeDtypeStruct((rows, cols), BF16),
        in_specs=[hbm] * 7 + [vmem] * 5,
        out_specs=vmem,
        scratch_shapes=scratch,
        compiler_params=pltpu.CompilerParams(
            collective_id=0, has_side_effects=True, vmem_limit_bytes=48 << 20
        ),
        name="layers",
    )(
        starting_stream,
        multiplier_matrix,
        memory_path_matrix,
        exit_projector_matrix,
        memory_valve_matrix,
        entry_valve_matrix,
        spike_extra,
        filter_coefficients,
        forgetting_parameters,
        timestep_forgetting_multiplier.reshape(1, rows),
        prelude_rms_gains,
        finishing_rms_gains.reshape(1, cols),
    )


def solution(mesh):
    return jax.shard_map(
        functools.partial(on_device, mesh.shape["sp"], mesh.shape["tp"]),
        mesh=mesh,
        in_specs=(
            P(("grp", "sp"), "tp"),
            P(None, "sp", "tp"),
            P(None, "sp", "tp"),
            P(None, None, "tp"),
            P(None, "tp", None, None),
            P(None, "tp", None, None),
            P(None, "tp"),
            P(("grp", "sp")),
            P(("grp", "sp"), "tp"),
            P(None, "tp", "sp"),
            P(),
            P("tp"),
        ),
        out_specs=P(("grp", "sp"), "tp"),
        check_vma=False,
    )
```

time: 604 us -> 203 us (0.34)
  waiting for transfers between devices: 271 us -> 0 us
  Pallas kernels: 0 us -> 195 us
  blocking collectives: 183 us -> 0 us
  starting transfers between devices: 52.9 us -> 0 us
  local copies, waits for them, and re-layouts: 42.2 us -> 8.36 us
  other arithmetic: 24.4 us -> 0 us
  between operations: 14.8 us -> 0.06 us
  matrix products: 13.7 us -> 0 us
    all_gather x4 -> x0, waiting for transfers between devices: 230 us -> none  [the longest x2 125 us: in_one_piece(): whole = lax.all_gather(both, axis, axis=dim, tiled=True)]
    pallas_call x0 -> x1, Pallas kernels: none -> 195 us  [on_device(): pl.pallas_call(functools.partial(kernel, n_sp, n_x), out_shape=jax.ShapeD...]
    all_to_all x3 -> x0, blocking collectives: 101 us -> none  [the longest x2 92.9 us: summed_on_arrival(): lax.all_to_all(tiles, axis, split_axis=0, concat_axis=0, tiled=True)]
    all_gather x2 -> x0, blocking collectives: 82.5 us -> none  [gathered_once(): both, at, found = (lax.all_gather(jnp.concatenate(lines), axis), 0, {})]
    all_to_all x2 -> x0, starting transfers between devices: 49.6 us -> none  [sent_to_all(): return lax.all_to_all(copies, axis, split_axis=0, concat_axis=0, tiled=True)]
    all_to_all x2 -> x0, waiting for transfers between devices: 38.8 us -> none  [sent_to_all(): return lax.all_to_all(copies, axis, split_axis=0, concat_axis=0, tiled=True)]
    slice x120 -> x0, local copies, waits for them, and re-layouts: 29.9 us -> none  [the longest x114 28.4 us: on_device(): lax.associative_scan(combine_pairs, (keep_rate, driven), axis=0)]
    dot_general x8 -> x0, matrix products: 13.7 us -> none  [the longest x2 7.69 us: on_device(): jnp.dot(mixed_in, out_full, preferred_element_type=jnp.float32)]
  transfers between devices with their start and end apart: 8 -> 0, of which waited for: 8 -> 0; matrix products, arithmetic and copies ran while one was open for 12% -> 0% of each run, Pallas kernels for 0% -> 0%
where the time goes in v1:
time: 203 us
  Pallas kernels  195 us (96%)
  local copies, waits for them, and re-layouts  8.36 us (4%)
    pallas_call x1, Pallas kernels, on_device(): pl.pallas_call(functools.partial(kernel, n_sp, n_x), out_shape=jax.ShapeD...  195 us
    unnamed x22, local copies, waits for them, and re-layouts  7.64 us

profile of v1, /device:TPU:33, one launch (start us, length us, event | category | flops | bytes accessed | tf_op | source)
XLA Modules:
  0.0 202.9 jit_solution(15059009170286580592)
XLA Ops:
  0.0 0.0 copy-start.3
  0.0 0.7 reshape.6.tm_ref
  0.7 0.0 copy-start.7
  0.7 0.0 copy-start.9
  0.7 1.0 copy.13.ex_hbm
  1.7 0.0 copy-done.3
  1.7 0.0 copy-done.7
  1.7 0.0 copy-done.9
  1.8 0.0 copy-start
  1.8 1.0 copy-done
  2.8 0.0 copy-start.1
  2.8 0.9 copy-done.1
  3.7 0.0 copy-start.2
  3.7 0.9 copy-done.2
  4.7 0.0 copy-start.4
  4.7 0.8 copy-done.4
  5.5 0.0 copy-start.5
  5.5 0.8 copy-done.5
  6.3 0.0 copy-start.6
  6.3 0.7 copy-done.6
  7.0 0.0 copy-start.8
  7.1 0.7 copy-done.8
  7.7 194.5 %layers.1 = bf16[384,256]{1,0:T(8,128)(2,1)S(1)} custom-call(bf16[384,256]{1,0:T(8,128)(2,1)S(1)} %copy-done.3, bf16[2,64,256]{2,1,0:T(8,128)(2,1)S(1)} %copy-done.4, bf16[2,64,256]{2,1,0:T(8,128)(2,1)S(1)} %copy-done.5, bf16[2,256,64]{2,1,0:T(8,128)(2,1)S(1)} %copy.13.ex_hbm, bf16[2,1,256,256]{3,2,1,0:T(8,128)(2,1)S(1)} %copy-done.1, ...), custom_call_target="tpu_custom_call" | custom-call | tf_op jit(solution)/shard_map/layers/pallas_call | solution.py:626
  202.3 0.7 copy.15
Async XLA Ops:
  0.0 1.7 copy-start.3
  0.7 1.0 copy-start.7
  0.7 1.0 copy-start.9
  1.8 1.0 copy-start
  2.8 0.9 copy-start.1
  3.7 0.9 copy-start.2
  4.7 0.8 copy-start.4
  5.5 0.8 copy-start.5
  6.3 0.7 copy-start.6
  7.0 0.7 copy-start.8
